TPU v7x, 32 devices: a whole 2x2x4 slice. The times are simulated.
32 devices in a mesh: pp: 2 (over x), fs: 4 (over y, core), tp: 4 (over z).
Axes of the slice: x: 2, y: 2, z: 4, core: 2. Of those that a mesh axis runs over, the one named last changes fastest.
Arguments:
- inputs: bfloat16 [512, 2048], P('pp', ('fs', 'tp')), may hold values from -6 to 6
- norm_gain: bfloat16 [2, 2048], P('pp', ('fs', 'tp')), may hold values from 0.099609375 to 1.8984375
- w_value: bfloat16 [2, 2048, 2048], P('pp', None, ('fs', 'tp')), may hold values from -0.125 to 0.125
- w_gate: bfloat16 [2, 2048, 2048], P('pp', None, ('fs', 'tp')), may hold values from -0.125 to 0.125
- w_taps: bfloat16 [2, 31, 2048], P('pp', None, ('fs', 'tp')), may hold values from -1 to 1
- ln_gain: float32 [2, 2048], P('pp', ('fs', 'tp')), may hold values from 0.1 to 1.9
- ln_shift: float32 [2, 2048], P('pp', ('fs', 'tp')), may hold values from -3 to 3
Outputs:
- outputs: bfloat16 [512, 2048], P('pp', ('fs', 'tp'))
All inputs are finite; a program needn't handle non-finite values.
Results may differ from a plain program's by a relative error of at most 0.0085.
Values may be sent and summed in bfloat16 or wider, within the bound.
A program may use at most 64 MiB of HBM per device.

v0:
```python
import jax
import jax.numpy as jnp
from jax import lax
from jax.sharding import PartitionSpec as P

LEN = 128
norm_eps = 1e-06
layer_eps = 1e-05


def from_behind(block, axis, distance):
    devices = range(lax.axis_size(axis))
    route = [(i - distance, i) for i in devices if i - distance in devices]
    return lax.ppermute(block, axis, route)


def local(inputs, norm_gain, w_value, w_gate, w_taps, ln_gain, ln_shift):
    num_sections = lax.axis_size("pp")
    my_section = lax.axis_index("pp")
    model_width = w_value.shape[1]
    channels = w_value.shape[2]
    tap_count = w_taps.shape[1]
    fed_rows = lax.all_gather(inputs, "pp", axis=0, tiled=True)
    total_rows = fed_rows.shape[0]
    block_rows = LEN
    per_batch = LEN // block_rows
    block_count = total_rows // block_rows
    step_count = block_count + num_sections - 1
    gain_row = norm_gain[0]
    value_weight = w_value[0]
    gate_weight = w_gate[0]
    tap_weights = w_taps[0].astype(jnp.float32)
    layer_gain = ln_gain[0]
    layer_shift = ln_shift[0]

    def convolve(operands):
        history, gated_rows = operands
        padded = jnp.concatenate([history, gated_rows], axis=0)
        convolved = jnp.zeros((block_rows, channels), jnp.float32)
        for tap_index in range(tap_count):
            convolved = (
                convolved + padded[tap_index : tap_index + block_rows] * tap_weights[tap_index]
            )
        return convolved

    def skip_convolve(operands):
        return jnp.zeros((block_rows, channels), jnp.float32)

    def process_block(stream, history, active):
        stream_f = stream.astype(jnp.float32)
        zero_block = jnp.zeros((block_rows, channels), jnp.float32)
        squares = lax.psum(jnp.sum(stream_f * stream_f, axis=1), ("fs", "tp"))
        scale_rows = lax.rsqrt(squares / model_width + norm_eps)[:, None]
        normed = (stream_f * scale_rows * gain_row.astype(jnp.float32)).astype(jnp.bfloat16)
        shard_piece = lax.all_gather(normed, ("fs", "tp"), axis=1, tiled=True)

        def accumulate(current):
            return (
                jnp.dot(shard_piece, value_weight, preferred_element_type=jnp.float32),
                jnp.dot(shard_piece, gate_weight, preferred_element_type=jnp.float32),
            )

        def unchanged(current):
            return current

        value_sum, gate_sum = lax.cond(active, accumulate, unchanged, (zero_block, zero_block))
        gated_rows = value_sum * jax.nn.sigmoid(gate_sum)
        convolved = lax.cond(active, convolve, skip_convolve, (history, gated_rows))
        new_history = jnp.where(
            active, jnp.concatenate([history, gated_rows], axis=0)[block_rows:], history
        )
        moments = lax.psum(
            (jnp.sum(convolved, axis=1), jnp.sum(convolved * convolved, axis=1)), ("fs", "tp")
        )
        row_mean = moments[0][:, None] / model_width
        row_var = moments[1][:, None] / model_width - row_mean * row_mean
        normed_conv = (convolved - row_mean) * lax.rsqrt(
            row_var + layer_eps
        ) * layer_gain + layer_shift
        new_stream = (stream_f + jax.nn.silu(normed_conv)).astype(jnp.bfloat16)
        return (jnp.where(active, new_stream, stream), new_history)

    def step_body(step_index, loop_state):
        stream, history, results = loop_state
        block_index = step_index - my_section
        active = (block_index >= 0) & (block_index < block_count)
        safe_index = jnp.clip(block_index, 0, block_count - 1)
        row_offset = safe_index * block_rows
        first_rows = lax.dynamic_slice_in_dim(fed_rows, row_offset, block_rows, 0)
        stream = jnp.where(my_section == 0, first_rows, stream)
        history = jnp.where(
            active & (safe_index % per_batch == 0), jnp.zeros_like(history), history
        )
        new_stream, new_history = process_block(stream, history, active)
        previous = lax.dynamic_slice_in_dim(results, row_offset, block_rows, 0)
        keep_rows = active & (my_section == num_sections - 1)
        results = lax.dynamic_update_slice_in_dim(
            results, jnp.where(keep_rows, new_stream, previous), row_offset, 0
        )
        passed = from_behind(new_stream, "pp", 1)
        return (passed, new_history, results)

    initial = (
        jnp.zeros((block_rows, channels), jnp.bfloat16),
        jnp.zeros((tap_count - 1, channels), jnp.float32),
        jnp.zeros((total_rows, channels), jnp.bfloat16),
    )
    final_state = lax.fori_loop(0, step_count, step_body, initial)
    own_rows = inputs.shape[0]
    shares = final_state[2].reshape(num_sections, own_rows, channels)
    arrived = lax.all_to_all(shares, "pp", split_axis=0, concat_axis=0, tiled=True)
    return arrived[num_sections - 1]


def solution(mesh):
    in_specs = (
        P("pp", ("fs", "tp")),
        P("pp", ("fs", "tp")),
        P("pp", None, ("fs", "tp")),
        P("pp", None, ("fs", "tp")),
        P("pp", None, ("fs", "tp")),
        P("pp", ("fs", "tp")),
        P("pp", ("fs", "tp")),
    )
    out_specs = P("pp", ("fs", "tp"))
    return jax.shard_map(local, mesh=mesh, in_specs=in_specs, out_specs=out_specs, check_vma=False)
```

profile of v0, /device:TPU:0, one launch (start us, length us, event | category | flops | bytes accessed | tf_op | source)
XLA Modules:
  0.0 539.6 jit_solution(15302463253678728073)
XLA Ops:
  0.0 6.3 %all_gather.13 = bf16[512,128]{1,0:T(8,128)(2,1)S(1)} all-gather(bf16[256,128]{1,0:T(8,128)(2,1)} %param.13), channel_id=1, replica_groups=mesh['pp'=2,'fs'=4,'tp'=4] {'pp'}, dimensions={0}, use_global_device_ids=true | all-gather | bytes 196608 | tf_op jit(solution)/shard_map/all_gather | solution.py:23
  7.0 524.0 %while.20 = (s32[]{:T(128)}, bf16[128,128]{1,0:T(8,128)(2,1)S(1)}, f32[30,128]{1,0:T(8,128)S(1)}, bf16[512,128]{1,0:T(8,128)(2,1)S(1)}, s32[]{:T(128)}, /*index=...) while((s32[]{:T(128)}, bf16[128,128]{1,0:T(8,128)(2,1)S(1)}, ...), condition=%wide.region_11.12_spmd.clone, body=%wide.region_0.11_spmd.clone.sunk | while | flops 136179984 | bytes 5903558 | solution.py:108
  7.1 33.1 %psum.46 = f32[128]{0:T(128)S(1)} all-reduce(f32[128]{0:T(128)S(1)} %get-tuple-element.554), channel_id=1, replica_groups=mesh['pp'=2,'fs'=4,'tp'=4] {'fs','tp'}, use_global_device_ids=true, to_apply=%region_2.2 | all-reduce | flops 128 | bytes 1024 | tf_op jit(solution)/shard_map/while/body/eval_jaxpr/psum | solution.py:52
  40.3 33.2 %all_gather.16 = bf16[128,2048]{1,0:T(8,128)(2,1)S(1)} all-gather(bf16[128,128]{1,0:T(8,128)(2,1)S(1)} %fusion.106), channel_id=1, replica_groups=mesh['pp'=2,'fs'=4,'tp'=4] {'fs','tp'}, dimensions={1}, use_global_device_ids=true | all-gather | bytes 557056 | tf_op jit(solution)/shard_map/while/body/eval_jaxpr/all_gather | solution.py:55
  75.6 31.4 %all-reduce.2 = (f32[128]{0:T(128)S(1)}, f32[128]{0:T(128)S(1)}) all-reduce(f32[128]{0:T(128)S(1)} %get-tuple-element.558, f32[128]{0:T(128)S(1)} %get-tuple-element.559), channel_id=1, replica_groups=mesh['pp'=2,'fs'=4,'tp'=4] {'fs','tp'}, use_global_device_ids=true, to_apply=%region_10.10 | all-reduce | flops 256 | bytes 2048 | tf_op jit(solution)/shard_map/while/body/eval_jaxpr/psum | solution.py:72
  107.1 1.7 collective-permute-start
  110.5 30.2 %psum.46 = f32[128]{0:T(128)S(1)} all-reduce(f32[128]{0:T(128)S(1)} %get-tuple-element.554), channel_id=1, replica_groups=mesh['pp'=2,'fs'=4,'tp'=4] {'fs','tp'}, use_global_device_ids=true, to_apply=%region_2.2 | all-reduce | flops 128 | bytes 1024 | tf_op jit(solution)/shard_map/while/body/eval_jaxpr/psum | solution.py:52
  140.8 36.4 %all_gather.16 = bf16[128,2048]{1,0:T(8,128)(2,1)S(1)} all-gather(bf16[128,128]{1,0:T(8,128)(2,1)S(1)} %fusion.106), channel_id=1, replica_groups=mesh['pp'=2,'fs'=4,'tp'=4] {'fs','tp'}, dimensions={1}, use_global_device_ids=true | all-gather | bytes 557056 | tf_op jit(solution)/shard_map/while/body/eval_jaxpr/all_gather | solution.py:55
  179.2 29.7 %all-reduce.2 = (f32[128]{0:T(128)S(1)}, f32[128]{0:T(128)S(1)}) all-reduce(f32[128]{0:T(128)S(1)} %get-tuple-element.558, f32[128]{0:T(128)S(1)} %get-tuple-element.559), channel_id=1, replica_groups=mesh['pp'=2,'fs'=4,'tp'=4] {'fs','tp'}, use_global_device_ids=true, to_apply=%region_10.10 | all-reduce | flops 256 | bytes 2048 | tf_op jit(solution)/shard_map/while/body/eval_jaxpr/psum | solution.py:72
  209.1 4.2 collective-permute-start
  215.0 32.0 %psum.46 = f32[128]{0:T(128)S(1)} all-reduce(f32[128]{0:T(128)S(1)} %get-tuple-element.554), channel_id=1, replica_groups=mesh['pp'=2,'fs'=4,'tp'=4] {'fs','tp'}, use_global_device_ids=true, to_apply=%region_2.2 | all-reduce | flops 128 | bytes 1024 | tf_op jit(solution)/shard_map/while/body/eval_jaxpr/psum | solution.py:52
  247.1 33.5 %all_gather.16 = bf16[128,2048]{1,0:T(8,128)(2,1)S(1)} all-gather(bf16[128,128]{1,0:T(8,128)(2,1)S(1)} %fusion.106), channel_id=1, replica_groups=mesh['pp'=2,'fs'=4,'tp'=4] {'fs','tp'}, dimensions={1}, use_global_device_ids=true | all-gather | bytes 557056 | tf_op jit(solution)/shard_map/while/body/eval_jaxpr/all_gather | solution.py:55
  282.7 32.0 %all-reduce.2 = (f32[128]{0:T(128)S(1)}, f32[128]{0:T(128)S(1)}) all-reduce(f32[128]{0:T(128)S(1)} %get-tuple-element.558, f32[128]{0:T(128)S(1)} %get-tuple-element.559), channel_id=1, replica_groups=mesh['pp'=2,'fs'=4,'tp'=4] {'fs','tp'}, use_global_device_ids=true, to_apply=%region_10.10 | all-reduce | flops 256 | bytes 2048 | tf_op jit(solution)/shard_map/while/body/eval_jaxpr/psum | solution.py:72
  314.8 4.2 collective-permute-start
  320.8 29.8 %psum.46 = f32[128]{0:T(128)S(1)} all-reduce(f32[128]{0:T(128)S(1)} %get-tuple-element.554), channel_id=1, replica_groups=mesh['pp'=2,'fs'=4,'tp'=4] {'fs','tp'}, use_global_device_ids=true, to_apply=%region_2.2 | all-reduce | flops 128 | bytes 1024 | tf_op jit(solution)/shard_map/while/body/eval_jaxpr/psum | solution.py:52
  350.7 36.8 %all_gather.16 = bf16[128,2048]{1,0:T(8,128)(2,1)S(1)} all-gather(bf16[128,128]{1,0:T(8,128)(2,1)S(1)} %fusion.106), channel_id=1, replica_groups=mesh['pp'=2,'fs'=4,'tp'=4] {'fs','tp'}, dimensions={1}, use_global_device_ids=true | all-gather | bytes 557056 | tf_op jit(solution)/shard_map/while/body/eval_jaxpr/all_gather | solution.py:55
  389.6 29.7 %all-reduce.2 = (f32[128]{0:T(128)S(1)}, f32[128]{0:T(128)S(1)}) all-reduce(f32[128]{0:T(128)S(1)} %get-tuple-element.558, f32[128]{0:T(128)S(1)} %get-tuple-element.559), channel_id=1, replica_groups=mesh['pp'=2,'fs'=4,'tp'=4] {'fs','tp'}, use_global_device_ids=true, to_apply=%region_10.10 | all-reduce | flops 256 | bytes 2048 | tf_op jit(solution)/shard_map/while/body/eval_jaxpr/psum | solution.py:72
  419.5 4.2 collective-permute-start
  425.4 32.0 %psum.46 = f32[128]{0:T(128)S(1)} all-reduce(f32[128]{0:T(128)S(1)} %get-tuple-element.554), channel_id=1, replica_groups=mesh['pp'=2,'fs'=4,'tp'=4] {'fs','tp'}, use_global_device_ids=true, to_apply=%region_2.2 | all-reduce | flops 128 | bytes 1024 | tf_op jit(solution)/shard_map/while/body/eval_jaxpr/psum | solution.py:52
  457.5 33.3 %all_gather.16 = bf16[128,2048]{1,0:T(8,128)(2,1)S(1)} all-gather(bf16[128,128]{1,0:T(8,128)(2,1)S(1)} %fusion.106), channel_id=1, replica_groups=mesh['pp'=2,'fs'=4,'tp'=4] {'fs','tp'}, dimensions={1}, use_global_device_ids=true | all-gather | bytes 557056 | tf_op jit(solution)/shard_map/while/body/eval_jaxpr/all_gather | solution.py:55
  491.1 32.0 %all-reduce.2 = (f32[128]{0:T(128)S(1)}, f32[128]{0:T(128)S(1)}) all-reduce(f32[128]{0:T(128)S(1)} %get-tuple-element.558, f32[128]{0:T(128)S(1)} %get-tuple-element.559), channel_id=1, replica_groups=mesh['pp'=2,'fs'=4,'tp'=4] {'fs','tp'}, use_global_device_ids=true, to_apply=%region_10.10 | all-reduce | flops 256 | bytes 2048 | tf_op jit(solution)/shard_map/while/body/eval_jaxpr/psum | solution.py:72
  523.2 6.1 %collective-permute-start = (bf16[128,128]{1,0:T(8,128)(2,1)S(1)}, bf16[128,128]{1,0:T(8,128)(2,1)S(1)}, u32[]{:S(2)}, u32[]{:S(2)}) collective-permute-start(bf16[128,128]{1,0:T(8,128)(2,1)S(1)} %get-tuple-element.564), channel_id=1, source_target_pairs={{0,16},{1,17},{2,18},{3,19},{4,20},{5,21},{6,22},{7,23},{8,24},{9,... | collective-permute-start | bytes 98312 | tf_op jit(solution)/shard_map/while/body/eval_jaxpr/ppermute | solution.py:14
  529.3 1.7 collective-permute-done
  531.0 8.0 %all_to_all.5 = bf16[2,256,128]{2,1,0:T(8,128)(2,1)S(1)} all-to-all(bf16[2,256,128]{2,1,0:T(8,128)(2,1)S(1)} %bitcast.83), channel_id=1, replica_groups=mesh['pp'=2,'fs'=4,'tp'=4] {'pp'}, dimensions={0} | all-to-all | bytes 262144 | tf_op jit(solution)/shard_map/all_to_all | solution.py:111
  (105 shorter events, 25.3 us)
Async XLA Ops:
  0.0 6.3 %copy-start.3 = (bf16[1,31,128]{2,1,0:T(8,128)(2,1)S(1)}, bf16[1,31,128]{2,1,0:T(8,128)(2,1)}, u32[]{:S(2)}) copy-start(bf16[1,31,128]{2,1,0:T(8,128)(2,1)} %param.17) | copy-start | bytes 23812
  6.3 0.7 copy-start.1
  6.3 0.7 copy-start.2
  6.3 0.7 copy-start.4
  7.0 66.5 %copy-start = (bf16[2048,128]{1,0:T(8,128)(2,1)S(1)}, bf16[2048,128]{1,0:T(8,128)(2,1)}, u32[]{:S(2)}) copy-start(bf16[2048,128]{1,0:T(8,128)(2,1)} %get-tuple-element.619) | copy-start | bytes 1572868 | tf_op jit(solution)/shard_map/while
  107.1 3.2 collective-permute-start
  110.4 66.8 %copy-start = (bf16[2048,128]{1,0:T(8,128)(2,1)S(1)}, bf16[2048,128]{1,0:T(8,128)(2,1)}, u32[]{:S(2)}) copy-start(bf16[2048,128]{1,0:T(8,128)(2,1)} %get-tuple-element.619) | copy-start | bytes 1572868 | tf_op jit(solution)/shard_map/while
  209.1 5.8 %collective-permute-start = (bf16[128,128]{1,0:T(8,128)(2,1)S(1)}, bf16[128,128]{1,0:T(8,128)(2,1)S(1)}, u32[]{:S(2)}, u32[]{:S(2)}) collective-permute-start(bf16[128,128]{1,0:T(8,128)(2,1)S(1)} %get-tuple-element.564), channel_id=1, source_target_pairs={{0,16},{1,17},{2,18},{3,19},{4,20},{5,21},{6,22},{7,23},{8,24},{9,... | collective-permute-start | bytes 98312 | tf_op jit(solution)/shard_map/while/body/eval_jaxpr/ppermute | solution.py:14
  214.9 65.7 %copy-start = (bf16[2048,128]{1,0:T(8,128)(2,1)S(1)}, bf16[2048,128]{1,0:T(8,128)(2,1)}, u32[]{:S(2)}) copy-start(bf16[2048,128]{1,0:T(8,128)(2,1)} %get-tuple-element.619) | copy-start | bytes 1572868 | tf_op jit(solution)/shard_map/while
  314.8 5.8 %collective-permute-start = (bf16[128,128]{1,0:T(8,128)(2,1)S(1)}, bf16[128,128]{1,0:T(8,128)(2,1)S(1)}, u32[]{:S(2)}, u32[]{:S(2)}) collective-permute-start(bf16[128,128]{1,0:T(8,128)(2,1)S(1)} %get-tuple-element.564), channel_id=1, source_target_pairs={{0,16},{1,17},{2,18},{3,19},{4,20},{5,21},{6,22},{7,23},{8,24},{9,... | collective-permute-start | bytes 98312 | tf_op jit(solution)/shard_map/while/body/eval_jaxpr/ppermute | solution.py:14
  320.6 66.9 %copy-start = (bf16[2048,128]{1,0:T(8,128)(2,1)S(1)}, bf16[2048,128]{1,0:T(8,128)(2,1)}, u32[]{:S(2)}) copy-start(bf16[2048,128]{1,0:T(8,128)(2,1)} %get-tuple-element.619) | copy-start | bytes 1572868 | tf_op jit(solution)/shard_map/while
  419.5 5.8 %collective-permute-start = (bf16[128,128]{1,0:T(8,128)(2,1)S(1)}, bf16[128,128]{1,0:T(8,128)(2,1)S(1)}, u32[]{:S(2)}, u32[]{:S(2)}) collective-permute-start(bf16[128,128]{1,0:T(8,128)(2,1)S(1)} %get-tuple-element.564), channel_id=1, source_target_pairs={{0,16},{1,17},{2,18},{3,19},{4,20},{5,21},{6,22},{7,23},{8,24},{9,... | collective-permute-start | bytes 98312 | tf_op jit(solution)/shard_map/while/body/eval_jaxpr/ppermute | solution.py:14
  425.3 65.6 %copy-start = (bf16[2048,128]{1,0:T(8,128)(2,1)S(1)}, bf16[2048,128]{1,0:T(8,128)(2,1)}, u32[]{:S(2)}) copy-start(bf16[2048,128]{1,0:T(8,128)(2,1)} %get-tuple-element.619) | copy-start | bytes 1572868 | tf_op jit(solution)/shard_map/while
  523.2 7.8 %collective-permute-start = (bf16[128,128]{1,0:T(8,128)(2,1)S(1)}, bf16[128,128]{1,0:T(8,128)(2,1)S(1)}, u32[]{:S(2)}, u32[]{:S(2)}) collective-permute-start(bf16[128,128]{1,0:T(8,128)(2,1)S(1)} %get-tuple-element.564), channel_id=1, source_target_pairs={{0,16},{1,17},{2,18},{3,19},{4,20},{5,21},{6,22},{7,23},{8,24},{9,... | collective-permute-start | bytes 98312 | tf_op jit(solution)/shard_map/while/body/eval_jaxpr/ppermute | solution.py:14
where the time goes:
time: 540 us
  blocking collectives  499 us (92%)
  starting transfers between devices  20.4 us (4%)
  waiting for transfers between devices  8.02 us (1%)
  matrix products  6.45 us (1%)
    all_gather x5, blocking collectives, process_block(): shard_piece = lax.all_gather(normed, ('fs', 'tp'), axis=1, tiled=True)  173 us
    psum x5, blocking collectives, process_block(): squares = lax.psum(jnp.sum(stream_f * stream_f, axis=1), ('fs', 'tp'))  157 us
    psum x5, blocking collectives, process_block(): lax.psum((jnp.sum(convolved, axis=1), jnp.sum(convolved * convolved, axis...  155 us
    ppermute x5, starting transfers between devices, from_behind(): return lax.ppermute(block, axis, route)  20.4 us
  transfers between devices with their start and end apart: 5, of which 5 were waited for; matrix products, arithmetic and copies ran while one was open for 0% of the time, Pallas kernels for 0%

commit v1 on v0

--- a/solution.py
+++ b/solution.py
@@ -69,9 +69,9 @@
         new_history = jnp.where(
             active, jnp.concatenate([history, gated_rows], axis=0)[block_rows:], history
         )
-        moments = lax.psum(
-            (jnp.sum(convolved, axis=1), jnp.sum(convolved * convolved, axis=1)), ("fs", "tp")
-        )
+        moments = (jnp.sum(convolved, axis=1), jnp.sum(convolved * convolved, axis=1))
+        for mesh_axis in ("tp", "fs"):
+            moments = lax.psum(moments, mesh_axis)
         row_mean = moments[0][:, None] / model_width
         row_var = moments[1][:, None] / model_width - row_mean * row_mean
         normed_conv = (convolved - row_mean) * lax.rsqrt(

time: 540 us -> 462 us (0.86)
  blocking collectives: 499 us -> 421 us
    psum x5 -> x10, blocking collectives: 155 us -> 76.4 us  [process_block(): moments = lax.psum(moments, mesh_axis)]
where the time goes in v1:
time: 462 us; the launch traced here: 461 us
  blocking collectives  421 us (91%)
  starting transfers between devices  20.6 us (4%)
  waiting for transfers between devices  7.87 us (2%)
  matrix products  6.46 us (1%)
    all_gather x5, blocking collectives, process_block(): shard_piece = lax.all_gather(normed, ('fs', 'tp'), axis=1, tiled=True)  174 us
    psum x5, blocking collectives, process_block(): squares = lax.psum(jnp.sum(stream_f * stream_f, axis=1), ('fs', 'tp'))  156 us
    psum x10, blocking collectives, process_block(): moments = lax.psum(moments, mesh_axis)  76.4 us
    ppermute x5, starting transfers between devices, from_behind(): return lax.ppermute(block, axis, route)  20.6 us
  transfers between devices with their start and end apart: 5, of which 5 were waited for; matrix products, arithmetic and copies ran while one was open for 0% of the time, Pallas kernels for 0%

profile of v1, /device:TPU:0, one launch (start us, length us, event | category | flops | bytes accessed | tf_op | source)
XLA Modules:
  0.0 461.1 jit_solution(4075061676413383717)
XLA Ops:
  0.0 6.3 %all_gather.13 = bf16[512,128]{1,0:T(8,128)(2,1)S(1)} all-gather(bf16[256,128]{1,0:T(8,128)(2,1)} %param.13), channel_id=1, replica_groups=mesh['pp'=2,'fs'=4,'tp'=4] {'pp'}, dimensions={0}, use_global_device_ids=true | all-gather | bytes 196608 | tf_op jit(solution)/shard_map/all_gather | solution.py:23
  7.0 445.6 %while.20 = (s32[]{:T(128)}, bf16[128,128]{1,0:T(8,128)(2,1)S(1)}, f32[30,128]{1,0:T(8,128)S(1)}, bf16[512,128]{1,0:T(8,128)(2,1)S(1)}, s32[]{:T(128)}, /*index=...) while((s32[]{:T(128)}, bf16[128,128]{1,0:T(8,128)(2,1)S(1)}, ...), condition=%wide.region_13.14_spmd.clone, body=%wide.region_0.13_spmd.clone.sunk | while | flops 136180240 | bytes 5905606 | solution.py:108
  7.1 33.1 %psum.76 = f32[128]{0:T(128)S(1)} all-reduce(f32[128]{0:T(128)S(1)} %get-tuple-element.558), channel_id=1, replica_groups=mesh['pp'=2,'fs'=4,'tp'=4] {'fs','tp'}, use_global_device_ids=true, to_apply=%region_2.2 | all-reduce | flops 128 | bytes 1024 | tf_op jit(solution)/shard_map/while/body/eval_jaxpr/psum | solution.py:52
  40.3 33.2 %all_gather.16 = bf16[128,2048]{1,0:T(8,128)(2,1)S(1)} all-gather(bf16[128,128]{1,0:T(8,128)(2,1)S(1)} %fusion.106), channel_id=1, replica_groups=mesh['pp'=2,'fs'=4,'tp'=4] {'fs','tp'}, dimensions={1}, use_global_device_ids=true | all-gather | bytes 557056 | tf_op jit(solution)/shard_map/while/body/eval_jaxpr/all_gather | solution.py:55
  75.6 10.1 %all-reduce.4 = (f32[128]{0:T(128)S(1)}, f32[128]{0:T(128)S(1)}) all-reduce(f32[128]{0:T(128)S(1)} %get-tuple-element.562, f32[128]{0:T(128)S(1)} %get-tuple-element.563), channel_id=1, replica_groups=mesh['pp'=2,'fs'=4,'tp'=4] {'tp'}, use_global_device_ids=true, to_apply=%region_11.11 | all-reduce | flops 256 | bytes 2048 | tf_op jit(solution)/shard_map/while/body/eval_jaxpr/psum | solution.py:74
  85.7 5.6 %all-reduce.5 = (f32[128]{0:T(128)S(1)}, f32[128]{0:T(128)S(1)}) all-reduce(f32[128]{0:T(128)S(1)} %get-tuple-element.564, f32[128]{0:T(128)S(1)} %get-tuple-element.565), channel_id=1, replica_groups=mesh['pp'=2,'fs'=4,'tp'=4] {'fs'}, use_global_device_ids=true, to_apply=%region_12.12 | all-reduce | flops 256 | bytes 2048 | tf_op jit(solution)/shard_map/while/body/eval_jaxpr/psum | solution.py:74
  94.9 29.9 %psum.76 = f32[128]{0:T(128)S(1)} all-reduce(f32[128]{0:T(128)S(1)} %get-tuple-element.558), channel_id=1, replica_groups=mesh['pp'=2,'fs'=4,'tp'=4] {'fs','tp'}, use_global_device_ids=true, to_apply=%region_2.2 | all-reduce | flops 128 | bytes 1024 | tf_op jit(solution)/shard_map/while/body/eval_jaxpr/psum | solution.py:52
  124.8 36.9 %all_gather.16 = bf16[128,2048]{1,0:T(8,128)(2,1)S(1)} all-gather(bf16[128,128]{1,0:T(8,128)(2,1)S(1)} %fusion.106), channel_id=1, replica_groups=mesh['pp'=2,'fs'=4,'tp'=4] {'fs','tp'}, dimensions={1}, use_global_device_ids=true | all-gather | bytes 557056 | tf_op jit(solution)/shard_map/while/body/eval_jaxpr/all_gather | solution.py:55
  163.8 8.4 %all-reduce.4 = (f32[128]{0:T(128)S(1)}, f32[128]{0:T(128)S(1)}) all-reduce(f32[128]{0:T(128)S(1)} %get-tuple-element.562, f32[128]{0:T(128)S(1)} %get-tuple-element.563), channel_id=1, replica_groups=mesh['pp'=2,'fs'=4,'tp'=4] {'tp'}, use_global_device_ids=true, to_apply=%region_11.11 | all-reduce | flops 256 | bytes 2048 | tf_op jit(solution)/shard_map/while/body/eval_jaxpr/psum | solution.py:74
  172.2 5.6 %all-reduce.5 = (f32[128]{0:T(128)S(1)}, f32[128]{0:T(128)S(1)}) all-reduce(f32[128]{0:T(128)S(1)} %get-tuple-element.564, f32[128]{0:T(128)S(1)} %get-tuple-element.565), channel_id=1, replica_groups=mesh['pp'=2,'fs'=4,'tp'=4] {'fs'}, use_global_device_ids=true, to_apply=%region_12.12 | all-reduce | flops 256 | bytes 2048 | tf_op jit(solution)/shard_map/while/body/eval_jaxpr/psum | solution.py:74
  183.9 31.8 %psum.76 = f32[128]{0:T(128)S(1)} all-reduce(f32[128]{0:T(128)S(1)} %get-tuple-element.558), channel_id=1, replica_groups=mesh['pp'=2,'fs'=4,'tp'=4] {'fs','tp'}, use_global_device_ids=true, to_apply=%region_2.2 | all-reduce | flops 128 | bytes 1024 | tf_op jit(solution)/shard_map/while/body/eval_jaxpr/psum | solution.py:52
  215.8 33.5 %all_gather.16 = bf16[128,2048]{1,0:T(8,128)(2,1)S(1)} all-gather(bf16[128,128]{1,0:T(8,128)(2,1)S(1)} %fusion.106), channel_id=1, replica_groups=mesh['pp'=2,'fs'=4,'tp'=4] {'fs','tp'}, dimensions={1}, use_global_device_ids=true | all-gather | bytes 557056 | tf_op jit(solution)/shard_map/while/body/eval_jaxpr/all_gather | solution.py:55
  251.4 10.7 %all-reduce.4 = (f32[128]{0:T(128)S(1)}, f32[128]{0:T(128)S(1)}) all-reduce(f32[128]{0:T(128)S(1)} %get-tuple-element.562, f32[128]{0:T(128)S(1)} %get-tuple-element.563), channel_id=1, replica_groups=mesh['pp'=2,'fs'=4,'tp'=4] {'tp'}, use_global_device_ids=true, to_apply=%region_11.11 | all-reduce | flops 256 | bytes 2048 | tf_op jit(solution)/shard_map/while/body/eval_jaxpr/psum | solution.py:74
  262.1 5.6 %all-reduce.5 = (f32[128]{0:T(128)S(1)}, f32[128]{0:T(128)S(1)}) all-reduce(f32[128]{0:T(128)S(1)} %get-tuple-element.564, f32[128]{0:T(128)S(1)} %get-tuple-element.565), channel_id=1, replica_groups=mesh['pp'=2,'fs'=4,'tp'=4] {'fs'}, use_global_device_ids=true, to_apply=%region_12.12 | all-reduce | flops 256 | bytes 2048 | tf_op jit(solution)/shard_map/while/body/eval_jaxpr/psum | solution.py:74
  273.9 29.8 %psum.76 = f32[128]{0:T(128)S(1)} all-reduce(f32[128]{0:T(128)S(1)} %get-tuple-element.558), channel_id=1, replica_groups=mesh['pp'=2,'fs'=4,'tp'=4] {'fs','tp'}, use_global_device_ids=true, to_apply=%region_2.2 | all-reduce | flops 128 | bytes 1024 | tf_op jit(solution)/shard_map/while/body/eval_jaxpr/psum | solution.py:52
  303.8 36.6 %all_gather.16 = bf16[128,2048]{1,0:T(8,128)(2,1)S(1)} all-gather(bf16[128,128]{1,0:T(8,128)(2,1)S(1)} %fusion.106), channel_id=1, replica_groups=mesh['pp'=2,'fs'=4,'tp'=4] {'fs','tp'}, dimensions={1}, use_global_device_ids=true | all-gather | bytes 557056 | tf_op jit(solution)/shard_map/while/body/eval_jaxpr/all_gather | solution.py:55
  342.5 8.4 %all-reduce.4 = (f32[128]{0:T(128)S(1)}, f32[128]{0:T(128)S(1)}) all-reduce(f32[128]{0:T(128)S(1)} %get-tuple-element.562, f32[128]{0:T(128)S(1)} %get-tuple-element.563), channel_id=1, replica_groups=mesh['pp'=2,'fs'=4,'tp'=4] {'tp'}, use_global_device_ids=true, to_apply=%region_11.11 | all-reduce | flops 256 | bytes 2048 | tf_op jit(solution)/shard_map/while/body/eval_jaxpr/psum | solution.py:74
  350.9 5.6 %all-reduce.5 = (f32[128]{0:T(128)S(1)}, f32[128]{0:T(128)S(1)}) all-reduce(f32[128]{0:T(128)S(1)} %get-tuple-element.564, f32[128]{0:T(128)S(1)} %get-tuple-element.565), channel_id=1, replica_groups=mesh['pp'=2,'fs'=4,'tp'=4] {'fs'}, use_global_device_ids=true, to_apply=%region_12.12 | all-reduce | flops 256 | bytes 2048 | tf_op jit(solution)/shard_map/while/body/eval_jaxpr/psum | solution.py:74
  362.6 31.8 %psum.76 = f32[128]{0:T(128)S(1)} all-reduce(f32[128]{0:T(128)S(1)} %get-tuple-element.558), channel_id=1, replica_groups=mesh['pp'=2,'fs'=4,'tp'=4] {'fs','tp'}, use_global_device_ids=true, to_apply=%region_2.2 | all-reduce | flops 128 | bytes 1024 | tf_op jit(solution)/shard_map/while/body/eval_jaxpr/psum | solution.py:52
  394.5 33.6 %all_gather.16 = bf16[128,2048]{1,0:T(8,128)(2,1)S(1)} all-gather(bf16[128,128]{1,0:T(8,128)(2,1)S(1)} %fusion.106), channel_id=1, replica_groups=mesh['pp'=2,'fs'=4,'tp'=4] {'fs','tp'}, dimensions={1}, use_global_device_ids=true | all-gather | bytes 557056 | tf_op jit(solution)/shard_map/while/body/eval_jaxpr/all_gather | solution.py:55
  428.4 10.7 %all-reduce.4 = (f32[128]{0:T(128)S(1)}, f32[128]{0:T(128)S(1)}) all-reduce(f32[128]{0:T(128)S(1)} %get-tuple-element.562, f32[128]{0:T(128)S(1)} %get-tuple-element.563), channel_id=1, replica_groups=mesh['pp'=2,'fs'=4,'tp'=4] {'tp'}, use_global_device_ids=true, to_apply=%region_11.11 | all-reduce | flops 256 | bytes 2048 | tf_op jit(solution)/shard_map/while/body/eval_jaxpr/psum | solution.py:74
  439.1 5.6 %all-reduce.5 = (f32[128]{0:T(128)S(1)}, f32[128]{0:T(128)S(1)}) all-reduce(f32[128]{0:T(128)S(1)} %get-tuple-element.564, f32[128]{0:T(128)S(1)} %get-tuple-element.565), channel_id=1, replica_groups=mesh['pp'=2,'fs'=4,'tp'=4] {'fs'}, use_global_device_ids=true, to_apply=%region_12.12 | all-reduce | flops 256 | bytes 2048 | tf_op jit(solution)/shard_map/while/body/eval_jaxpr/psum | solution.py:74
  444.9 6.1 %collective-permute-start = (bf16[128,128]{1,0:T(8,128)(2,1)S(1)}, bf16[128,128]{1,0:T(8,128)(2,1)S(1)}, u32[]{:S(2)}, u32[]{:S(2)}) collective-permute-start(bf16[128,128]{1,0:T(8,128)(2,1)S(1)} %get-tuple-element.570), channel_id=1, source_target_pairs={{0,16},{1,17},{2,18},{3,19},{4,20},{5,21},{6,22},{7,23},{8,24},{9,... | collective-permute-start | bytes 98312 | tf_op jit(solution)/shard_map/while/body/eval_jaxpr/ppermute | solution.py:14
  452.6 7.8 %all_to_all.5 = bf16[2,256,128]{2,1,0:T(8,128)(2,1)S(1)} all-to-all(bf16[2,256,128]{2,1,0:T(8,128)(2,1)S(1)} %bitcast.83), channel_id=1, replica_groups=mesh['pp'=2,'fs'=4,'tp'=4] {'pp'}, dimensions={0} | all-to-all | bytes 262144 | tf_op jit(solution)/shard_map/all_to_all | solution.py:111
  (110 shorter events, 41.3 us)
Async XLA Ops:
  0.0 6.3 %copy-start.3 = (bf16[1,31,128]{2,1,0:T(8,128)(2,1)S(1)}, bf16[1,31,128]{2,1,0:T(8,128)(2,1)}, u32[]{:S(2)}) copy-start(bf16[1,31,128]{2,1,0:T(8,128)(2,1)} %param.17) | copy-start | bytes 23812
  6.3 0.7 copy-start.1
  6.3 0.7 copy-start.2
  6.3 0.7 copy-start.4
  7.0 66.5 %copy-start = (bf16[2048,128]{1,0:T(8,128)(2,1)S(1)}, bf16[2048,128]{1,0:T(8,128)(2,1)}, u32[]{:S(2)}) copy-start(bf16[2048,128]{1,0:T(8,128)(2,1)} %get-tuple-element.625) | copy-start | bytes 1572868 | tf_op jit(solution)/shard_map/while
  91.5 3.3 collective-permute-start
  94.7 67.0 %copy-start = (bf16[2048,128]{1,0:T(8,128)(2,1)S(1)}, bf16[2048,128]{1,0:T(8,128)(2,1)}, u32[]{:S(2)}) copy-start(bf16[2048,128]{1,0:T(8,128)(2,1)} %get-tuple-element.625) | copy-start | bytes 1572868 | tf_op jit(solution)/shard_map/while
  178.0 5.8 %collective-permute-start = (bf16[128,128]{1,0:T(8,128)(2,1)S(1)}, bf16[128,128]{1,0:T(8,128)(2,1)S(1)}, u32[]{:S(2)}, u32[]{:S(2)}) collective-permute-start(bf16[128,128]{1,0:T(8,128)(2,1)S(1)} %get-tuple-element.570), channel_id=1, source_target_pairs={{0,16},{1,17},{2,18},{3,19},{4,20},{5,21},{6,22},{7,23},{8,24},{9,... | collective-permute-start | bytes 98312 | tf_op jit(solution)/shard_map/while/body/eval_jaxpr/ppermute | solution.py:14
  183.8 65.5 %copy-start = (bf16[2048,128]{1,0:T(8,128)(2,1)S(1)}, bf16[2048,128]{1,0:T(8,128)(2,1)}, u32[]{:S(2)}) copy-start(bf16[2048,128]{1,0:T(8,128)(2,1)} %get-tuple-element.625) | copy-start | bytes 1572868 | tf_op jit(solution)/shard_map/while
  267.9 5.9 %collective-permute-start = (bf16[128,128]{1,0:T(8,128)(2,1)S(1)}, bf16[128,128]{1,0:T(8,128)(2,1)S(1)}, u32[]{:S(2)}, u32[]{:S(2)}) collective-permute-start(bf16[128,128]{1,0:T(8,128)(2,1)S(1)} %get-tuple-element.570), channel_id=1, source_target_pairs={{0,16},{1,17},{2,18},{3,19},{4,20},{5,21},{6,22},{7,23},{8,24},{9,... | collective-permute-start | bytes 98312 | tf_op jit(solution)/shard_map/while/body/eval_jaxpr/ppermute | solution.py:14
  273.8 66.6 %copy-start = (bf16[2048,128]{1,0:T(8,128)(2,1)S(1)}, bf16[2048,128]{1,0:T(8,128)(2,1)}, u32[]{:S(2)}) copy-start(bf16[2048,128]{1,0:T(8,128)(2,1)} %get-tuple-element.625) | copy-start | bytes 1572868 | tf_op jit(solution)/shard_map/while
  356.7 5.8 %collective-permute-start = (bf16[128,128]{1,0:T(8,128)(2,1)S(1)}, bf16[128,128]{1,0:T(8,128)(2,1)S(1)}, u32[]{:S(2)}, u32[]{:S(2)}) collective-permute-start(bf16[128,128]{1,0:T(8,128)(2,1)S(1)} %get-tuple-element.570), channel_id=1, source_target_pairs={{0,16},{1,17},{2,18},{3,19},{4,20},{5,21},{6,22},{7,23},{8,24},{9,... | collective-permute-start | bytes 98312 | tf_op jit(solution)/shard_map/while/body/eval_jaxpr/ppermute | solution.py:14
  362.5 65.7 %copy-start = (bf16[2048,128]{1,0:T(8,128)(2,1)S(1)}, bf16[2048,128]{1,0:T(8,128)(2,1)}, u32[]{:S(2)}) copy-start(bf16[2048,128]{1,0:T(8,128)(2,1)} %get-tuple-element.625) | copy-start | bytes 1572868 | tf_op jit(solution)/shard_map/while
  444.9 7.7 %collective-permute-start = (bf16[128,128]{1,0:T(8,128)(2,1)S(1)}, bf16[128,128]{1,0:T(8,128)(2,1)S(1)}, u32[]{:S(2)}, u32[]{:S(2)}) collective-permute-start(bf16[128,128]{1,0:T(8,128)(2,1)S(1)} %get-tuple-element.570), channel_id=1, source_target_pairs={{0,16},{1,17},{2,18},{3,19},{4,20},{5,21},{6,22},{7,23},{8,24},{9,... | collective-permute-start | bytes 98312 | tf_op jit(solution)/shard_map/while/body/eval_jaxpr/ppermute | solution.py:14
